TPU v7x, 32 devices: a whole 2x2x4 slice. The times are simulated.
32 devices in a mesh: pp: 4 (over y, x), tp: 8 (over z, core).
Axes of the slice: x: 2, y: 2, z: 4, core: 2. Of those that a mesh axis runs over, the one named last changes fastest.
Arguments:
- entry_stream_rows: bfloat16 [256, 2048], P('pp', 'tp'), may hold values from -21 to 21
- layer_rescale_factor: float32 [4, 2048], P('pp'), may hold values from 0.1 to 1.9
- probe_projection: bfloat16 [4, 2048, 2048], P('pp', 'tp'), may hold values from -0.125 to 0.125
- retention_projection: bfloat16 [4, 2048, 2048], P('pp', 'tp'), may hold values from -0.125 to 0.125
- candidate_projection: bfloat16 [4, 2048, 2048], P('pp', 'tp'), may hold values from -0.125 to 0.125
- emission_filter_matrix: bfloat16 [4, 2048, 2048], P('pp', 'tp'), may hold values from -0.125 to 0.125
- retention_minimum: float32 [4, 2048], P('pp', 'tp'), may hold values from 0.88 to 0.9921875
- decay_spike: float32 [4, 128, 32], P('pp', None, 'tp'), may hold values from -2.1 to 0
- per_group_scale: float32 [4, 64], P('pp'), may hold values from 0.1 to 1.9
Outputs:
- outputs: bfloat16 [256, 2048], P('pp', 'tp')
All inputs are finite; a program needn't handle non-finite values.
Results may differ from a plain program's by a relative error of at most 0.03.
Values may be sent and summed in bfloat16 or wider, within the bound.
A program may use at most 64 MiB of HBM per device.

v0:
```python
import jax
import jax.numpy as jnp
from jax import lax
from jax.sharding import PartitionSpec as P

HEAD = 64
SEG = 64
EPSILON = 1e-06
HIGHEST = lax.Precision.HIGHEST


def shifted(array, axis, by):
    devices = lax.axis_size(axis)
    pairs = [(i, i + by) for i in range(devices) if 0 <= i + by < devices]
    return lax.ppermute(array, axis, pairs)


def spread(value, axis, source):
    kept = jnp.where(lax.axis_index(axis) == source, value, 0).astype(value.dtype)
    return lax.psum(kept, axis)


def segment_scan(queries, key_in, log_forget, values, memory):
    head_count = queries.shape[0]
    length = queries.shape[1]
    blocks_count = length // SEG

    def split_blocks(tensor):
        return tensor.reshape(head_count, blocks_count, SEG, tensor.shape[-1]).transpose(1, 0, 2, 3)

    lower_mask = jnp.tril(jnp.ones((SEG, SEG), dtype=bool))[None]

    def one_block(memory_in, pieces):
        block_query, block_key, block_forget, block_value = pieces
        running = jnp.cumsum(block_forget, axis=1)
        query_scaled = block_query * jnp.exp(running)
        key_scaled = block_key * jnp.exp(-running)
        scores = jnp.einsum("hid,hjd->hij", query_scaled, key_scaled, precision=HIGHEST)
        scores = jnp.where(lower_mask, scores, 0.0)
        mixed_out = jnp.einsum("hij,hjv->hiv", scores, block_value, precision=HIGHEST)
        mixed_out = mixed_out + jnp.einsum(
            "hid,hdv->hiv", query_scaled, memory_in, precision=HIGHEST
        )
        ending = running[:, -1:, :]
        carried_in = jnp.einsum(
            "hjd,hjv->hdv", block_key * jnp.exp(ending - running), block_value, precision=HIGHEST
        )
        memory_out = jnp.exp(ending[:, 0, :])[:, :, None] * memory_in + carried_in
        return (memory_out, mixed_out)

    memory, mixed_out = lax.scan(
        one_block,
        memory,
        (
            split_blocks(queries),
            split_blocks(key_in),
            split_blocks(log_forget),
            split_blocks(values),
        ),
    )
    return (mixed_out.transpose(1, 0, 2, 3).reshape(head_count, length, values.shape[-1]), memory)


def head_norm(mixed_out, channel_gain):
    return (
        mixed_out
        * lax.rsqrt(jnp.mean(mixed_out * mixed_out, axis=-1, keepdims=True) + EPSILON)
        * channel_gain
    )


def shards(
    entry_stream_rows,
    layer_rescale_factor,
    probe_projection,
    retention_projection,
    candidate_projection,
    emission_filter_matrix,
    retention_minimum,
    decay_spike,
    per_group_scale,
):
    sections = lax.axis_size("pp")
    layer_ordinal = lax.axis_index("pp")
    own_rows = entry_stream_rows.shape[0]
    seq_len = 2 * own_rows
    columns = entry_stream_rows.shape[1]
    head_here = columns // HEAD
    model_width = layer_rescale_factor.shape[1]
    micro_count = sections // 2
    per_sequence = seq_len // seq_len
    unit_count = micro_count * per_sequence
    total_steps = unit_count + sections - 1
    entering = lax.all_gather(entry_stream_rows, "pp", axis=0, tiled=True)
    weights = jnp.concatenate(
        [
            probe_projection[0],
            retention_projection[0],
            candidate_projection[0],
            emission_filter_matrix[0],
        ],
        axis=0,
    )
    input_gain = layer_rescale_factor[0]
    lower_edge = retention_minimum[0].reshape(head_here, 1, HEAD)
    spike_collection = decay_spike[0].T
    out_gain = per_group_scale[0]

    def add_piece(piece_in):
        wide_piece = piece_in.astype(jnp.float32)
        scaled = (wide_piece * input_gain[None, :]).astype(jnp.bfloat16)
        product = lax.dot_general(
            scaled, weights, (((1,), (1,)), ((), ())), preferred_element_type=jnp.float32
        )
        return (product, jnp.sum(wide_piece * wide_piece, axis=1))

    def one_step(step_index, carried):
        incoming, memory, finished = carried
        unit_index = step_index - layer_ordinal
        first_slot = jnp.clip(step_index, 0, unit_count - 1)
        fresh_rows = lax.dynamic_slice_in_dim(entering, first_slot * seq_len, seq_len, 0)
        current = jnp.where(layer_ordinal == 0, fresh_rows, incoming)
        projected, squares = add_piece(lax.all_gather(current, "tp", axis=1, tiled=True))
        inverse = lax.rsqrt(squares / model_width + EPSILON)[:, None]
        projected = projected * inverse

        def per_head(role_index):
            picked = projected[:, role_index * columns : (role_index + 1) * columns]
            return picked.reshape(seq_len, head_here, HEAD).transpose(1, 0, 2)

        query_pre = per_head(0)
        forget_pre = per_head(1)
        input_pre = per_head(2)
        gate_pre = per_head(3)
        offset = unit_index % per_sequence * seq_len
        current_surge = spike_collection[:, :, None]
        log_forget = (
            jnp.logaddexp(
                jnp.log(lower_edge), jnp.log1p(-lower_edge) + jax.nn.log_sigmoid(forget_pre)
            )
            + current_surge
        )
        key_in = (1.0 - lower_edge) * jax.nn.sigmoid(-forget_pre)
        queries = jax.nn.silu(query_pre)
        memory = jnp.where(offset == 0, jnp.zeros_like(memory), memory)
        mixed_out, memory = segment_scan(queries, key_in, log_forget, input_pre, memory)
        branch = head_norm(mixed_out, out_gain) * jax.nn.silu(gate_pre)
        branch = branch.transpose(1, 0, 2).reshape(seq_len, columns)
        result = (current.astype(jnp.float32) + branch).astype(jnp.bfloat16)
        passed = shifted(result, "pp", 1)
        out_slot = jnp.clip(unit_index, 0, unit_count - 1)
        write_here = (layer_ordinal == sections - 1) & (unit_index >= 0) & (unit_index < unit_count)
        updated = lax.dynamic_update_slice_in_dim(finished, result, out_slot * seq_len, 0)
        finished = jnp.where(write_here, updated, finished)
        return (passed, memory, finished)

    start_state = (
        jnp.zeros((seq_len, columns), jnp.bfloat16),
        jnp.zeros((head_here, HEAD, HEAD), jnp.float32),
        jnp.zeros((unit_count * seq_len, columns), jnp.bfloat16),
    )
    carried_out = lax.fori_loop(0, total_steps, one_step, start_state)
    everything = spread(carried_out[2], "pp", sections - 1)
    return lax.dynamic_slice_in_dim(everything, layer_ordinal * own_rows, own_rows, 0)


def solution(mesh):
    in_specs = (
        P("pp", "tp"),
        P("pp", None),
        P("pp", "tp", None),
        P("pp", "tp", None),
        P("pp", "tp", None),
        P("pp", "tp", None),
        P("pp", "tp"),
        P("pp", None, "tp"),
        P("pp", None),
    )
    out_specs = P("pp", "tp")
    return jax.shard_map(shards, mesh=mesh, in_specs=in_specs, out_specs=out_specs, check_vma=False)
```

profile of v0, /device:TPU:0, one launch (start us, length us, event | category | flops | bytes accessed | tf_op | source)
XLA Modules:
  0.0 245.3 jit_solution(12410205212231642517)
XLA Ops:
  6.5 0.6 broadcast.164
  7.1 1.4 reduce.10
  8.6 10.1 %all_gather.14 = bf16[256,256]{1,0:T(8,128)(2,1)S(1)} all-gather(bf16[64,256]{1,0:T(8,128)(2,1)} %param.13), channel_id=1, replica_groups=mesh['pp'=4,'tp'=8] {'pp'}, dimensions={0}, use_global_device_ids=true | all-gather | bytes 163840 | tf_op jit(solution)/shard_map/all_gather | solution.py:94
  18.8 3.7 %pad_maximum_fusion = bf16[1024,2048]{1,0:T(8,128)(2,1)} fusion(bf16[256,2048]{1,0:T(8,128)(2,1)} %bitcast.150, bf16[256,2048]{1,0:T(8,128)(2,1)} %bitcast.151, bf16[256,2048]{1,0:T(8,128)(2,1)} %bitcast.152, bf16[256,2048]{1,0:T(8,128)(2,1)} %bitcast.153), kind=kLoop, calls=%fused_computation.50 | loop fusion | flops 16777216 | bytes 8388608 | tf_op jit(solution)/shard_map/concatenate | solution.py:95
  22.5 167.6 %while.59 = (s32[]{:T(128)}, bf16[128,256]{0,1:T(8,128)(2,1)S(1)}, bf16[256,256]{1,0:T(8,128)(2,1)S(1)}, pred[]{:T(512)}, bf16[256,256]{1,0:T(8,128)(2,1)S(1)}, ...) while((s32[]{:T(128)}, bf16[128,256]{0,1:T(8,128)(2,1)S(1)}, ...), condition=%wide.region_6.7_spmd, body=%wide.region_0.6_spmd.sunk | while | flops 591418240 | bytes 15908739 | solution.py:162
  22.8 15.2 %all_gather.16 = bf16[128,2048]{0,1:T(8,128)(2,1)S(1)} all-gather(bf16[128,256]{0,1:T(8,128)(2,1)S(1)} %broadcast_select_fusion.5), channel_id=1, replica_groups=mesh['pp'=4,'tp'=8] {'tp'}, dimensions={1}, use_global_device_ids=true | all-gather | bytes 589824 | tf_op jit(solution)/shard_map/while/body/eval_jaxpr/all_gather | solution.py:123
  38.2 4.2 %convolution_multiply_fusion.2 = f32[128,1024]{1,0:T(8,128)S(1)} fusion(bf16[1024,2048]{1,0:T(8,128)(2,1)} %get-tuple-element.759, bf16[128,2048]{0,1:T(8,128)(2,1)S(1)} %all_gather.16, f32[2048]{0:T(1024)S(1)} %bitcast.154, f32[128]{0:T(128)S(1)} %add_rsqrt_fusion.4), kind=kOutput, calls=%fused_computation.26.clone.1 | convolution fusion | flops 537788416 | bytes 5251584 | tf_op jit(solution)/shard_map/while/body/eval_jaxpr/dot_general | solution.py:112
  44.0 5.0 %while.60 = (s32[]{:T(128)}, f32[4,64,64]{2,1,0:T(8,128)S(1)}, f32[2,4,64,64]{3,2,1,0:T(8,128)S(1)}, f32[2,4,64,64]{2,0,3,1:T(2,128)S(1)}, f32[2,4,64,64]{2,0,3,...) while((s32[]{:T(128)}, f32[4,64,64]{2,1,0:T(8,128)S(1)}, ...), condition=%wide.region_4.4_spmd.clone, body=%wide.region_2.3_spmd.clone.sunk | while | flops 51564544 | bytes 2504832 | solution.py:51
  45.0 0.4 convolution_select_fusion.2
  45.4 0.3 fusion.48
  46.1 0.4 convolution_add_fusion.3
  47.5 0.4 convolution_select_fusion.2
  47.9 0.3 fusion.48
  48.6 0.4 convolution_add_fusion.3
  50.0 3.2 %collective-permute-start = (bf16[128,256]{0,1:T(8,128)(2,1)S(1)}, bf16[128,256]{0,1:T(8,128)(2,1)S(1)}, u32[]{:S(2)}, u32[]{:S(2)}) collective-permute-start(bf16[128,256]{0,1:T(8,128)(2,1)S(1)} %get-tuple-element.665), channel_id=1, source_target_pairs={{0,8},{8,16},{16,24},{1,9},{9,17},{17,25},{2,10},{10,18},{18,26},{... | collective-permute-start | bytes 196616 | tf_op jit(solution)/shard_map/while/body/eval_jaxpr/ppermute | solution.py:15
  53.3 1.8 collective-permute-done
  55.2 14.7 %all_gather.16 = bf16[128,2048]{0,1:T(8,128)(2,1)S(1)} all-gather(bf16[128,256]{0,1:T(8,128)(2,1)S(1)} %broadcast_select_fusion.5), channel_id=1, replica_groups=mesh['pp'=4,'tp'=8] {'tp'}, dimensions={1}, use_global_device_ids=true | all-gather | bytes 589824 | tf_op jit(solution)/shard_map/while/body/eval_jaxpr/all_gather | solution.py:123
  70.2 4.2 %convolution_multiply_fusion.2 = f32[128,1024]{1,0:T(8,128)S(1)} fusion(bf16[1024,2048]{1,0:T(8,128)(2,1)} %get-tuple-element.759, bf16[128,2048]{0,1:T(8,128)(2,1)S(1)} %all_gather.16, f32[2048]{0:T(1024)S(1)} %bitcast.154, f32[128]{0:T(128)S(1)} %add_rsqrt_fusion.4), kind=kOutput, calls=%fused_computation.26.clone.1 | convolution fusion | flops 537788416 | bytes 5251584 | tf_op jit(solution)/shard_map/while/body/eval_jaxpr/dot_general | solution.py:112
  76.0 5.0 %while.60 = (s32[]{:T(128)}, f32[4,64,64]{2,1,0:T(8,128)S(1)}, f32[2,4,64,64]{3,2,1,0:T(8,128)S(1)}, f32[2,4,64,64]{2,0,3,1:T(2,128)S(1)}, f32[2,4,64,64]{2,0,3,...) while((s32[]{:T(128)}, f32[4,64,64]{2,1,0:T(8,128)S(1)}, ...), condition=%wide.region_4.4_spmd.clone, body=%wide.region_2.3_spmd.clone.sunk | while | flops 51564544 | bytes 2504832 | solution.py:51
  77.0 0.4 convolution_select_fusion.2
  77.4 0.3 fusion.48
  78.1 0.4 convolution_add_fusion.3
  79.5 0.4 convolution_select_fusion.2
  79.9 0.3 fusion.48
  80.6 0.4 convolution_add_fusion.3
  82.0 4.3 %collective-permute-start = (bf16[128,256]{0,1:T(8,128)(2,1)S(1)}, bf16[128,256]{0,1:T(8,128)(2,1)S(1)}, u32[]{:S(2)}, u32[]{:S(2)}) collective-permute-start(bf16[128,256]{0,1:T(8,128)(2,1)S(1)} %get-tuple-element.665), channel_id=1, source_target_pairs={{0,8},{8,16},{16,24},{1,9},{9,17},{17,25},{2,10},{10,18},{18,26},{... | collective-permute-start | bytes 196616 | tf_op jit(solution)/shard_map/while/body/eval_jaxpr/ppermute | solution.py:15
  86.5 1.8 collective-permute-done
  88.3 15.0 %all_gather.16 = bf16[128,2048]{0,1:T(8,128)(2,1)S(1)} all-gather(bf16[128,256]{0,1:T(8,128)(2,1)S(1)} %broadcast_select_fusion.5), channel_id=1, replica_groups=mesh['pp'=4,'tp'=8] {'tp'}, dimensions={1}, use_global_device_ids=true | all-gather | bytes 589824 | tf_op jit(solution)/shard_map/while/body/eval_jaxpr/all_gather | solution.py:123
  103.6 4.2 %convolution_multiply_fusion.2 = f32[128,1024]{1,0:T(8,128)S(1)} fusion(bf16[1024,2048]{1,0:T(8,128)(2,1)} %get-tuple-element.759, bf16[128,2048]{0,1:T(8,128)(2,1)S(1)} %all_gather.16, f32[2048]{0:T(1024)S(1)} %bitcast.154, f32[128]{0:T(128)S(1)} %add_rsqrt_fusion.4), kind=kOutput, calls=%fused_computation.26.clone.1 | convolution fusion | flops 537788416 | bytes 5251584 | tf_op jit(solution)/shard_map/while/body/eval_jaxpr/dot_general | solution.py:112
  109.4 5.0 %while.60 = (s32[]{:T(128)}, f32[4,64,64]{2,1,0:T(8,128)S(1)}, f32[2,4,64,64]{3,2,1,0:T(8,128)S(1)}, f32[2,4,64,64]{2,0,3,1:T(2,128)S(1)}, f32[2,4,64,64]{2,0,3,...) while((s32[]{:T(128)}, f32[4,64,64]{2,1,0:T(8,128)S(1)}, ...), condition=%wide.region_4.4_spmd.clone, body=%wide.region_2.3_spmd.clone.sunk | while | flops 51564544 | bytes 2504832 | solution.py:51
  110.5 0.4 convolution_select_fusion.2
  110.8 0.3 fusion.48
  111.5 0.4 convolution_add_fusion.3
  113.0 0.4 convolution_select_fusion.2
  113.3 0.3 fusion.48
  114.0 0.4 convolution_add_fusion.3
  115.4 4.3 %collective-permute-start = (bf16[128,256]{0,1:T(8,128)(2,1)S(1)}, bf16[128,256]{0,1:T(8,128)(2,1)S(1)}, u32[]{:S(2)}, u32[]{:S(2)}) collective-permute-start(bf16[128,256]{0,1:T(8,128)(2,1)S(1)} %get-tuple-element.665), channel_id=1, source_target_pairs={{0,8},{8,16},{16,24},{1,9},{9,17},{17,25},{2,10},{10,18},{18,26},{... | collective-permute-start | bytes 196616 | tf_op jit(solution)/shard_map/while/body/eval_jaxpr/ppermute | solution.py:15
  119.9 1.8 collective-permute-done
  121.8 14.9 %all_gather.16 = bf16[128,2048]{0,1:T(8,128)(2,1)S(1)} all-gather(bf16[128,256]{0,1:T(8,128)(2,1)S(1)} %broadcast_select_fusion.5), channel_id=1, replica_groups=mesh['pp'=4,'tp'=8] {'tp'}, dimensions={1}, use_global_device_ids=true | all-gather | bytes 589824 | tf_op jit(solution)/shard_map/while/body/eval_jaxpr/all_gather | solution.py:123
  137.0 4.2 %convolution_multiply_fusion.2 = f32[128,1024]{1,0:T(8,128)S(1)} fusion(bf16[1024,2048]{1,0:T(8,128)(2,1)} %get-tuple-element.759, bf16[128,2048]{0,1:T(8,128)(2,1)S(1)} %all_gather.16, f32[2048]{0:T(1024)S(1)} %bitcast.154, f32[128]{0:T(128)S(1)} %add_rsqrt_fusion.4), kind=kOutput, calls=%fused_computation.26.clone.1 | convolution fusion | flops 537788416 | bytes 5251584 | tf_op jit(solution)/shard_map/while/body/eval_jaxpr/dot_general | solution.py:112
  142.7 5.0 %while.60 = (s32[]{:T(128)}, f32[4,64,64]{2,1,0:T(8,128)S(1)}, f32[2,4,64,64]{3,2,1,0:T(8,128)S(1)}, f32[2,4,64,64]{2,0,3,1:T(2,128)S(1)}, f32[2,4,64,64]{2,0,3,...) while((s32[]{:T(128)}, f32[4,64,64]{2,1,0:T(8,128)S(1)}, ...), condition=%wide.region_4.4_spmd.clone, body=%wide.region_2.3_spmd.clone.sunk | while | flops 51564544 | bytes 2504832 | solution.py:51
  143.8 0.4 convolution_select_fusion.2
  144.1 0.3 fusion.48
  144.8 0.4 convolution_add_fusion.3
  146.3 0.4 convolution_select_fusion.2
  146.6 0.3 fusion.48
  147.3 0.4 convolution_add_fusion.3
  148.7 5.2 %collective-permute-start = (bf16[128,256]{0,1:T(8,128)(2,1)S(1)}, bf16[128,256]{0,1:T(8,128)(2,1)S(1)}, u32[]{:S(2)}, u32[]{:S(2)}) collective-permute-start(bf16[128,256]{0,1:T(8,128)(2,1)S(1)} %get-tuple-element.665), channel_id=1, source_target_pairs={{0,8},{8,16},{16,24},{1,9},{9,17},{17,25},{2,10},{10,18},{18,26},{... | collective-permute-start | bytes 196616 | tf_op jit(solution)/shard_map/while/body/eval_jaxpr/ppermute | solution.py:15
  154.0 1.8 collective-permute-done
  155.9 15.0 %all_gather.16 = bf16[128,2048]{0,1:T(8,128)(2,1)S(1)} all-gather(bf16[128,256]{0,1:T(8,128)(2,1)S(1)} %broadcast_select_fusion.5), channel_id=1, replica_groups=mesh['pp'=4,'tp'=8] {'tp'}, dimensions={1}, use_global_device_ids=true | all-gather | bytes 589824 | tf_op jit(solution)/shard_map/while/body/eval_jaxpr/all_gather | solution.py:123
  170.9 0.3 fusion.41
  171.2 4.2 %convolution_multiply_fusion.2 = f32[128,1024]{1,0:T(8,128)S(1)} fusion(bf16[1024,2048]{1,0:T(8,128)(2,1)} %get-tuple-element.759, bf16[128,2048]{0,1:T(8,128)(2,1)S(1)} %all_gather.16, f32[2048]{0:T(1024)S(1)} %bitcast.154, f32[128]{0:T(128)S(1)} %add_rsqrt_fusion.4), kind=kOutput, calls=%fused_computation.26.clone.1 | convolution fusion | flops 537788416 | bytes 5251584 | tf_op jit(solution)/shard_map/while/body/eval_jaxpr/dot_general | solution.py:112
  177.0 5.0 %while.60 = (s32[]{:T(128)}, f32[4,64,64]{2,1,0:T(8,128)S(1)}, f32[2,4,64,64]{3,2,1,0:T(8,128)S(1)}, f32[2,4,64,64]{2,0,3,1:T(2,128)S(1)}, f32[2,4,64,64]{2,0,3,...) while((s32[]{:T(128)}, f32[4,64,64]{2,1,0:T(8,128)S(1)}, ...), condition=%wide.region_4.4_spmd.clone, body=%wide.region_2.3_spmd.clone.sunk | while | flops 51564544 | bytes 2504832 | solution.py:51
  178.0 0.4 convolution_select_fusion.2
  178.4 0.3 fusion.48
  179.1 0.4 convolution_add_fusion.3
  180.5 0.4 convolution_select_fusion.2
  180.9 0.3 fusion.48
  181.5 0.4 convolution_add_fusion.3
  183.0 5.2 %collective-permute-start = (bf16[128,256]{0,1:T(8,128)(2,1)S(1)}, bf16[128,256]{0,1:T(8,128)(2,1)S(1)}, u32[]{:S(2)}, u32[]{:S(2)}) collective-permute-start(bf16[128,256]{0,1:T(8,128)(2,1)S(1)} %get-tuple-element.665), channel_id=1, source_target_pairs={{0,8},{8,16},{16,24},{1,9},{9,17},{17,25},{2,10},{10,18},{18,26},{... | collective-permute-start | bytes 196616 | tf_op jit(solution)/shard_map/while/body/eval_jaxpr/ppermute | solution.py:15
  188.3 1.8 collective-permute-done
  190.1 0.6 broadcast_select_fusion.2
  190.8 46.3 %all-reduce.2.cloned.1.call-done = bf16[256,256]{1,0:T(8,128)(2,1)} async-done(((bf16[256,256]{1,0:T(8,128)(2,1)}), bf16[256,256]{1,0:T(8,128)(2,1)}) %all-reduce.2.cloned.1.call-update) | async-done | bytes 131088 | tf_op jit(solution)/shard_map/psum | solution.py:20
  237.0 1.4 constant_dynamic-slice_fusion.6
  (276 shorter events, 27.5 us)
Async XLA Ops:
  6.5 230.5 %all-reduce.2.cloned.1.call-start = ((), (), s32[]{:S(2)}) async-start(), calls=%async_computation | async-start | bytes 262144 | tf_op jit(solution)/shard_map/psum | solution.py:20
  18.7 3.8 %copy-start = (f32[1,2048]{1,0:T(1,128)S(1)}, f32[1,2048]{1,0:T(1,128)}, u32[]{:S(2)}) copy-start(f32[1,2048]{1,0:T(1,128)} %param.14) | copy-start | bytes 24580
  18.7 3.8 %copy-start.1 = (f32[1,128,4]{1,2,0:T(4,128)S(1)}, f32[1,128,4]{1,2,0:T(4,128)}, u32[]{:S(2)}) copy-start(f32[1,128,4]{1,2,0:T(4,128)} %param.20) | copy-start | bytes 6148
  18.8 3.8 %copy-start.2 = (f32[1,64]{1,0:T(1,128)S(1)}, f32[1,64]{1,0:T(1,128)}, u32[]{:S(2)}) copy-start(f32[1,64]{1,0:T(1,128)} %param.21) | copy-start | bytes 772
  50.0 5.1 %collective-permute-start = (bf16[128,256]{0,1:T(8,128)(2,1)S(1)}, bf16[128,256]{0,1:T(8,128)(2,1)S(1)}, u32[]{:S(2)}, u32[]{:S(2)}) collective-permute-start(bf16[128,256]{0,1:T(8,128)(2,1)S(1)} %get-tuple-element.665), channel_id=1, source_target_pairs={{0,8},{8,16},{16,24},{1,9},{9,17},{17,25},{2,10},{10,18},{18,26},{... | collective-permute-start | bytes 196616 | tf_op jit(solution)/shard_map/while/body/eval_jaxpr/ppermute | solution.py:15
  82.0 6.2 %collective-permute-start = (bf16[128,256]{0,1:T(8,128)(2,1)S(1)}, bf16[128,256]{0,1:T(8,128)(2,1)S(1)}, u32[]{:S(2)}, u32[]{:S(2)}) collective-permute-start(bf16[128,256]{0,1:T(8,128)(2,1)S(1)} %get-tuple-element.665), channel_id=1, source_target_pairs={{0,8},{8,16},{16,24},{1,9},{9,17},{17,25},{2,10},{10,18},{18,26},{... | collective-permute-start | bytes 196616 | tf_op jit(solution)/shard_map/while/body/eval_jaxpr/ppermute | solution.py:15
  115.4 6.2 %collective-permute-start = (bf16[128,256]{0,1:T(8,128)(2,1)S(1)}, bf16[128,256]{0,1:T(8,128)(2,1)S(1)}, u32[]{:S(2)}, u32[]{:S(2)}) collective-permute-start(bf16[128,256]{0,1:T(8,128)(2,1)S(1)} %get-tuple-element.665), channel_id=1, source_target_pairs={{0,8},{8,16},{16,24},{1,9},{9,17},{17,25},{2,10},{10,18},{18,26},{... | collective-permute-start | bytes 196616 | tf_op jit(solution)/shard_map/while/body/eval_jaxpr/ppermute | solution.py:15
  148.7 7.1 %collective-permute-start = (bf16[128,256]{0,1:T(8,128)(2,1)S(1)}, bf16[128,256]{0,1:T(8,128)(2,1)S(1)}, u32[]{:S(2)}, u32[]{:S(2)}) collective-permute-start(bf16[128,256]{0,1:T(8,128)(2,1)S(1)} %get-tuple-element.665), channel_id=1, source_target_pairs={{0,8},{8,16},{16,24},{1,9},{9,17},{17,25},{2,10},{10,18},{18,26},{... | collective-permute-start | bytes 196616 | tf_op jit(solution)/shard_map/while/body/eval_jaxpr/ppermute | solution.py:15
  183.0 7.1 %collective-permute-start = (bf16[128,256]{0,1:T(8,128)(2,1)S(1)}, bf16[128,256]{0,1:T(8,128)(2,1)S(1)}, u32[]{:S(2)}, u32[]{:S(2)}) collective-permute-start(bf16[128,256]{0,1:T(8,128)(2,1)S(1)} %get-tuple-element.665), channel_id=1, source_target_pairs={{0,8},{8,16},{16,24},{1,9},{9,17},{17,25},{2,10},{10,18},{18,26},{... | collective-permute-start | bytes 196616 | tf_op jit(solution)/shard_map/while/body/eval_jaxpr/ppermute | solution.py:15
Sparse Core Ops, SparseCore 0:
  190.9 46.0 all-reduce.1
where the time goes:
time: 246 us; the launch traced here: 245 us
  blocking collectives  84.9 us (35%)
  waiting for transfers between devices  55 us (22%)
  matrix products  34.7 us (14%)
  starting transfers between devices  22.3 us (9%)
  local copies, waits for them, and re-layouts  20.5 us (8%)
  between operations  13.4 us (5%)
  other arithmetic  12.1 us (5%)
    all_gather x5, blocking collectives, one_step(): lax.all_gather(current, 'tp', axis=1, tiled=True)  74.8 us
    psum x1, waiting for transfers between devices, spread(): return lax.psum(kept, axis)  46.3 us
    ppermute x5, starting transfers between devices, shifted(): return lax.ppermute(array, axis, pairs)  22.3 us
    dot_general x5, matrix products, add_piece(): lax.dot_general(scaled, weights, (((1,), (1,)), ((), ())), preferred_elem...  20.8 us
    all_gather x1, blocking collectives, shards(): entering = lax.all_gather(entry_stream_rows, 'pp', axis=0, tiled=True)  10.1 us
    ppermute x5, waiting for transfers between devices, shifted(): return lax.ppermute(array, axis, pairs)  8.75 us
    dynamic_slice x50, local copies, waits for them, and re-layouts, segment_scan(): lax.scan(one_block, memory, (split_blocks(queries), split_blocks(key_in),...  8.32 us
  transfers between devices with their start and end apart: 6, of which 6 were waited for; matrix products, arithmetic and copies ran while one was open for 0% of the time, Pallas kernels for 0%

commit v1 on v0

--- a/solution.py
+++ b/solution.py
@@ -9,6 +9,12 @@
 HIGHEST = lax.Precision.HIGHEST
 
 
+def add_all(block, mesh_axis):
+    parts = lax.all_gather(block, mesh_axis, axis=0, tiled=False)
+    total = parts.sum(axis=0)
+    return total
+
+
 def shifted(array, axis, by):
     devices = lax.axis_size(axis)
     pairs = [(i, i + by) for i in range(devices) if 0 <= i + by < devices]
@@ -17,7 +23,7 @@
 
 def spread(value, axis, source):
     kept = jnp.where(lax.axis_index(axis) == source, value, 0).astype(value.dtype)
-    return lax.psum(kept, axis)
+    return add_all(kept, axis)
 
 
 def segment_scan(queries, key_in, log_forget, values, memory):

time: 246 us -> 201 us (0.82)
  waiting for transfers between devices: 55 us -> 9.41 us
  blocking collectives: 84.9 us -> 101 us
  between operations: 13.4 us -> 0.09 us
    psum x1 -> x0, waiting for transfers between devices: 46.3 us -> none  [spread(): return lax.psum(kept, axis)]
    all_gather x0 -> x1, blocking collectives: none -> 16.3 us  [add_all(): parts = lax.all_gather(block, mesh_axis, axis=0, tiled=False)]
  transfers between devices with their start and end apart: 6 -> 5, of which waited for: 6 -> 5; matrix products, arithmetic and copies ran while one was open for 0% -> 0% of each run, Pallas kernels for 0% -> 0%
where the time goes in v1:
time: 201 us
  blocking collectives  101 us (50%)
  matrix products  34.7 us (17%)
  starting transfers between devices  22.4 us (11%)
  local copies, waits for them, and re-layouts  19 us (9%)
  other arithmetic  12.2 us (6%)
  waiting for transfers between devices  9.41 us (5%)
  loops' own time  2.08 us (1%)
    all_gather x5, blocking collectives, one_step(): lax.all_gather(current, 'tp', axis=1, tiled=True)  74.8 us
    ppermute x5, starting transfers between devices, shifted(): return lax.ppermute(array, axis, pairs)  22.4 us
    dot_general x5, matrix products, add_piece(): lax.dot_general(scaled, weights, (((1,), (1,)), ((), ())), preferred_elem...  20.8 us
    all_gather x1, blocking collectives, add_all(): parts = lax.all_gather(block, mesh_axis, axis=0, tiled=False)  16.3 us
    all_gather x1, blocking collectives, shards(): entering = lax.all_gather(entry_stream_rows, 'pp', axis=0, tiled=True)  9.93 us
    ppermute x5, waiting for transfers between devices, shifted(): return lax.ppermute(array, axis, pairs)  9.41 us
    dynamic_slice x50, local copies, waits for them, and re-layouts, segment_scan(): lax.scan(one_block, memory, (split_blocks(queries), split_blocks(key_in),...  8.32 us
    dot_general x10, matrix products, one_block(): jnp.einsum('hjd,hjv->hdv', block_key * jnp.exp(ending - running), block_v...  4.14 us
  transfers between devices with their start and end apart: 5, of which 5 were waited for; matrix products, arithmetic and copies ran while one was open for 0% of the time, Pallas kernels for 0%

profile of v1, /device:TPU:0, one launch (start us, length us, event | category | flops | bytes accessed | tf_op | source)
XLA Modules:
  0.0 201.0 jit_solution(2899185413569783871)
XLA Ops:
  0.0 0.5 broadcast.164
  0.5 1.3 reduce.11
  2.0 3.7 %pad_maximum_fusion = bf16[1024,2048]{1,0:T(8,128)(2,1)} fusion(bf16[256,2048]{1,0:T(8,128)(2,1)} %bitcast.151, bf16[256,2048]{1,0:T(8,128)(2,1)} %bitcast.152, bf16[256,2048]{1,0:T(8,128)(2,1)} %bitcast.153, bf16[256,2048]{1,0:T(8,128)(2,1)} %bitcast.154), kind=kLoop, calls=%fused_computation.48 | loop fusion | flops 16777216 | bytes 8388608 | tf_op jit(solution)/shard_map/concatenate | solution.py:101
  5.7 9.9 %all_gather.20 = bf16[256,256]{1,0:T(8,128)(2,1)S(1)} all-gather(bf16[64,256]{1,0:T(8,128)(2,1)S(1)} %copy-done.2), channel_id=1, replica_groups=mesh['pp'=4,'tp'=8] {'pp'}, dimensions={0}, use_global_device_ids=true | all-gather | bytes 163840 | tf_op jit(solution)/shard_map/all_gather | solution.py:100
  15.7 167.1 %while.59 = (s32[]{:T(128)}, bf16[128,256]{0,1:T(8,128)(2,1)S(1)}, bf16[256,256]{0,1:T(8,128)(2,1)S(1)}, pred[]{:T(512)}, bf16[256,256]{1,0:T(8,128)(2,1)S(1)}, ...) while((s32[]{:T(128)}, bf16[128,256]{0,1:T(8,128)(2,1)S(1)}, ...), condition=%wide.region_6.7_spmd, body=%wide.region_0.6_spmd.sunk | while | flops 591418240 | bytes 15384447 | solution.py:168
  15.9 15.2 %all_gather.24 = bf16[128,2048]{0,1:T(8,128)(2,1)S(1)} all-gather(bf16[128,256]{0,1:T(8,128)(2,1)S(1)} %broadcast_select_fusion.3), channel_id=1, replica_groups=mesh['pp'=4,'tp'=8] {'tp'}, dimensions={1}, use_global_device_ids=true | all-gather | bytes 589824 | tf_op jit(solution)/shard_map/while/body/eval_jaxpr/all_gather | solution.py:129
  31.4 4.2 %convolution_multiply_fusion.2 = f32[128,1024]{1,0:T(8,128)S(1)} fusion(bf16[1024,2048]{1,0:T(8,128)(2,1)} %get-tuple-element.745, bf16[128,2048]{0,1:T(8,128)(2,1)S(1)} %all_gather.24, f32[2048]{0:T(1024)S(1)} %bitcast.155, f32[128]{0:T(128)S(1)} %add_rsqrt_fusion.4), kind=kOutput, calls=%fused_computation.26.clone.1 | convolution fusion | flops 537788416 | bytes 5251584 | tf_op jit(solution)/shard_map/while/body/eval_jaxpr/dot_general | solution.py:118
  37.1 5.0 %while.60 = (s32[]{:T(128)}, f32[4,64,64]{2,1,0:T(8,128)S(1)}, f32[2,4,64,64]{3,2,1,0:T(8,128)S(1)}, f32[2,4,64,64]{2,0,3,1:T(2,128)S(1)}, f32[2,4,64,64]{2,0,3,...) while((s32[]{:T(128)}, f32[4,64,64]{2,1,0:T(8,128)S(1)}, ...), condition=%wide.region_4.4_spmd.clone, body=%wide.region_2.3_spmd.clone.sunk | while | flops 51564544 | bytes 2504832 | solution.py:57
  38.2 0.4 convolution_select_fusion.2
  38.6 0.3 fusion.47
  39.2 0.4 convolution_add_fusion.3
  40.7 0.4 convolution_select_fusion.2
  41.0 0.3 fusion.47
  41.7 0.4 convolution_add_fusion.3
  43.0 3.4 %collective-permute-start = (bf16[128,256]{0,1:T(8,128)(2,1)S(1)}, bf16[128,256]{0,1:T(8,128)(2,1)S(1)}, u32[]{:S(2)}, u32[]{:S(2)}) collective-permute-start(bf16[128,256]{0,1:T(8,128)(2,1)S(1)} %get-tuple-element.651), channel_id=1, source_target_pairs={{0,8},{8,16},{16,24},{1,9},{9,17},{17,25},{2,10},{10,18},{18,26},{... | collective-permute-start | bytes 196616 | tf_op jit(solution)/shard_map/while/body/eval_jaxpr/ppermute | solution.py:21
  46.4 1.9 collective-permute-done
  48.4 14.7 %all_gather.24 = bf16[128,2048]{0,1:T(8,128)(2,1)S(1)} all-gather(bf16[128,256]{0,1:T(8,128)(2,1)S(1)} %broadcast_select_fusion.3), channel_id=1, replica_groups=mesh['pp'=4,'tp'=8] {'tp'}, dimensions={1}, use_global_device_ids=true | all-gather | bytes 589824 | tf_op jit(solution)/shard_map/while/body/eval_jaxpr/all_gather | solution.py:129
  63.4 4.2 %convolution_multiply_fusion.2 = f32[128,1024]{1,0:T(8,128)S(1)} fusion(bf16[1024,2048]{1,0:T(8,128)(2,1)} %get-tuple-element.745, bf16[128,2048]{0,1:T(8,128)(2,1)S(1)} %all_gather.24, f32[2048]{0:T(1024)S(1)} %bitcast.155, f32[128]{0:T(128)S(1)} %add_rsqrt_fusion.4), kind=kOutput, calls=%fused_computation.26.clone.1 | convolution fusion | flops 537788416 | bytes 5251584 | tf_op jit(solution)/shard_map/while/body/eval_jaxpr/dot_general | solution.py:118
  69.2 5.0 %while.60 = (s32[]{:T(128)}, f32[4,64,64]{2,1,0:T(8,128)S(1)}, f32[2,4,64,64]{3,2,1,0:T(8,128)S(1)}, f32[2,4,64,64]{2,0,3,1:T(2,128)S(1)}, f32[2,4,64,64]{2,0,3,...) while((s32[]{:T(128)}, f32[4,64,64]{2,1,0:T(8,128)S(1)}, ...), condition=%wide.region_4.4_spmd.clone, body=%wide.region_2.3_spmd.clone.sunk | while | flops 51564544 | bytes 2504832 | solution.py:57
  70.3 0.4 convolution_select_fusion.2
  70.6 0.3 fusion.47
  71.3 0.4 convolution_add_fusion.3
  72.8 0.4 convolution_select_fusion.2
  73.1 0.3 fusion.47
  73.8 0.4 convolution_add_fusion.3
  75.1 4.3 %collective-permute-start = (bf16[128,256]{0,1:T(8,128)(2,1)S(1)}, bf16[128,256]{0,1:T(8,128)(2,1)S(1)}, u32[]{:S(2)}, u32[]{:S(2)}) collective-permute-start(bf16[128,256]{0,1:T(8,128)(2,1)S(1)} %get-tuple-element.651), channel_id=1, source_target_pairs={{0,8},{8,16},{16,24},{1,9},{9,17},{17,25},{2,10},{10,18},{18,26},{... | collective-permute-start | bytes 196616 | tf_op jit(solution)/shard_map/while/body/eval_jaxpr/ppermute | solution.py:21
  79.4 1.9 collective-permute-done
  81.5 15.0 %all_gather.24 = bf16[128,2048]{0,1:T(8,128)(2,1)S(1)} all-gather(bf16[128,256]{0,1:T(8,128)(2,1)S(1)} %broadcast_select_fusion.3), channel_id=1, replica_groups=mesh['pp'=4,'tp'=8] {'tp'}, dimensions={1}, use_global_device_ids=true | all-gather | bytes 589824 | tf_op jit(solution)/shard_map/while/body/eval_jaxpr/all_gather | solution.py:129
  96.8 4.2 %convolution_multiply_fusion.2 = f32[128,1024]{1,0:T(8,128)S(1)} fusion(bf16[1024,2048]{1,0:T(8,128)(2,1)} %get-tuple-element.745, bf16[128,2048]{0,1:T(8,128)(2,1)S(1)} %all_gather.24, f32[2048]{0:T(1024)S(1)} %bitcast.155, f32[128]{0:T(128)S(1)} %add_rsqrt_fusion.4), kind=kOutput, calls=%fused_computation.26.clone.1 | convolution fusion | flops 537788416 | bytes 5251584 | tf_op jit(solution)/shard_map/while/body/eval_jaxpr/dot_general | solution.py:118
  102.5 5.0 %while.60 = (s32[]{:T(128)}, f32[4,64,64]{2,1,0:T(8,128)S(1)}, f32[2,4,64,64]{3,2,1,0:T(8,128)S(1)}, f32[2,4,64,64]{2,0,3,1:T(2,128)S(1)}, f32[2,4,64,64]{2,0,3,...) while((s32[]{:T(128)}, f32[4,64,64]{2,1,0:T(8,128)S(1)}, ...), condition=%wide.region_4.4_spmd.clone, body=%wide.region_2.3_spmd.clone.sunk | while | flops 51564544 | bytes 2504832 | solution.py:57
  103.6 0.4 convolution_select_fusion.2
  103.9 0.3 fusion.47
  104.6 0.4 convolution_add_fusion.3
  106.1 0.4 convolution_select_fusion.2
  106.4 0.3 fusion.47
  107.1 0.4 convolution_add_fusion.3
  108.4 4.3 %collective-permute-start = (bf16[128,256]{0,1:T(8,128)(2,1)S(1)}, bf16[128,256]{0,1:T(8,128)(2,1)S(1)}, u32[]{:S(2)}, u32[]{:S(2)}) collective-permute-start(bf16[128,256]{0,1:T(8,128)(2,1)S(1)} %get-tuple-element.651), channel_id=1, source_target_pairs={{0,8},{8,16},{16,24},{1,9},{9,17},{17,25},{2,10},{10,18},{18,26},{... | collective-permute-start | bytes 196616 | tf_op jit(solution)/shard_map/while/body/eval_jaxpr/ppermute | solution.py:21
  112.7 1.9 collective-permute-done
  114.7 15.0 %all_gather.24 = bf16[128,2048]{0,1:T(8,128)(2,1)S(1)} all-gather(bf16[128,256]{0,1:T(8,128)(2,1)S(1)} %broadcast_select_fusion.3), channel_id=1, replica_groups=mesh['pp'=4,'tp'=8] {'tp'}, dimensions={1}, use_global_device_ids=true | all-gather | bytes 589824 | tf_op jit(solution)/shard_map/while/body/eval_jaxpr/all_gather | solution.py:129
  130.0 4.2 %convolution_multiply_fusion.2 = f32[128,1024]{1,0:T(8,128)S(1)} fusion(bf16[1024,2048]{1,0:T(8,128)(2,1)} %get-tuple-element.745, bf16[128,2048]{0,1:T(8,128)(2,1)S(1)} %all_gather.24, f32[2048]{0:T(1024)S(1)} %bitcast.155, f32[128]{0:T(128)S(1)} %add_rsqrt_fusion.4), kind=kOutput, calls=%fused_computation.26.clone.1 | convolution fusion | flops 537788416 | bytes 5251584 | tf_op jit(solution)/shard_map/while/body/eval_jaxpr/dot_general | solution.py:118
  135.8 5.0 %while.60 = (s32[]{:T(128)}, f32[4,64,64]{2,1,0:T(8,128)S(1)}, f32[2,4,64,64]{3,2,1,0:T(8,128)S(1)}, f32[2,4,64,64]{2,0,3,1:T(2,128)S(1)}, f32[2,4,64,64]{2,0,3,...) while((s32[]{:T(128)}, f32[4,64,64]{2,1,0:T(8,128)S(1)}, ...), condition=%wide.region_4.4_spmd.clone, body=%wide.region_2.3_spmd.clone.sunk | while | flops 51564544 | bytes 2504832 | solution.py:57
  136.8 0.4 convolution_select_fusion.2
  137.2 0.3 fusion.47
  137.9 0.4 convolution_add_fusion.3
  139.3 0.4 convolution_select_fusion.2
  139.7 0.3 fusion.47
  140.4 0.4 convolution_add_fusion.3
  141.6 5.1 %collective-permute-start = (bf16[128,256]{0,1:T(8,128)(2,1)S(1)}, bf16[128,256]{0,1:T(8,128)(2,1)S(1)}, u32[]{:S(2)}, u32[]{:S(2)}) collective-permute-start(bf16[128,256]{0,1:T(8,128)(2,1)S(1)} %get-tuple-element.651), channel_id=1, source_target_pairs={{0,8},{8,16},{16,24},{1,9},{9,17},{17,25},{2,10},{10,18},{18,26},{... | collective-permute-start | bytes 196616 | tf_op jit(solution)/shard_map/while/body/eval_jaxpr/ppermute | solution.py:21
  146.8 1.9 collective-permute-done
  148.8 14.9 %all_gather.24 = bf16[128,2048]{0,1:T(8,128)(2,1)S(1)} all-gather(bf16[128,256]{0,1:T(8,128)(2,1)S(1)} %broadcast_select_fusion.3), channel_id=1, replica_groups=mesh['pp'=4,'tp'=8] {'tp'}, dimensions={1}, use_global_device_ids=true | all-gather | bytes 589824 | tf_op jit(solution)/shard_map/while/body/eval_jaxpr/all_gather | solution.py:129
  164.0 4.2 %convolution_multiply_fusion.2 = f32[128,1024]{1,0:T(8,128)S(1)} fusion(bf16[1024,2048]{1,0:T(8,128)(2,1)} %get-tuple-element.745, bf16[128,2048]{0,1:T(8,128)(2,1)S(1)} %all_gather.24, f32[2048]{0:T(1024)S(1)} %bitcast.155, f32[128]{0:T(128)S(1)} %add_rsqrt_fusion.4), kind=kOutput, calls=%fused_computation.26.clone.1 | convolution fusion | flops 537788416 | bytes 5251584 | tf_op jit(solution)/shard_map/while/body/eval_jaxpr/dot_general | solution.py:118
  169.8 5.0 %while.60 = (s32[]{:T(128)}, f32[4,64,64]{2,1,0:T(8,128)S(1)}, f32[2,4,64,64]{3,2,1,0:T(8,128)S(1)}, f32[2,4,64,64]{2,0,3,1:T(2,128)S(1)}, f32[2,4,64,64]{2,0,3,...) while((s32[]{:T(128)}, f32[4,64,64]{2,1,0:T(8,128)S(1)}, ...), condition=%wide.region_4.4_spmd.clone, body=%wide.region_2.3_spmd.clone.sunk | while | flops 51564544 | bytes 2504832 | solution.py:57
  170.8 0.4 convolution_select_fusion.2
  171.2 0.3 fusion.47
  171.9 0.4 convolution_add_fusion.3
  173.3 0.4 convolution_select_fusion.2
  173.7 0.3 fusion.47
  174.4 0.4 convolution_add_fusion.3
  175.7 5.2 %collective-permute-start = (bf16[128,256]{0,1:T(8,128)(2,1)S(1)}, bf16[128,256]{0,1:T(8,128)(2,1)S(1)}, u32[]{:S(2)}, u32[]{:S(2)}) collective-permute-start(bf16[128,256]{0,1:T(8,128)(2,1)S(1)} %get-tuple-element.651), channel_id=1, source_target_pairs={{0,8},{8,16},{16,24},{1,9},{9,17},{17,25},{2,10},{10,18},{18,26},{... | collective-permute-start | bytes 196616 | tf_op jit(solution)/shard_map/while/body/eval_jaxpr/ppermute | solution.py:21
  180.9 1.9 collective-permute-done
  182.8 16.3 %all-gather = bf16[1024,256]{0,1:T(8,128)(2,1)S(1)} all-gather(bf16[256,256]{0,1:T(8,128)(2,1)S(1)} %broadcast_select_fusion.1), channel_id=2, replica_groups=mesh['pp'=4,'tp'=8] {'pp'}, dimensions={0}, use_global_device_ids=true | all-gather | bytes 655360 | tf_op jit(solution)/shard_map/all_gather | solution.py:13
  199.1 0.4 reshape.200
  199.5 0.7 reduce_sum.40
  200.2 0.7 copy.50
  (259 shorter events, 26.7 us)
Async XLA Ops:
  2.0 3.8 %copy-start.2 = (bf16[64,256]{1,0:T(8,128)(2,1)S(1)}, bf16[64,256]{1,0:T(8,128)(2,1)}, u32[]{:S(2)}) copy-start(bf16[64,256]{1,0:T(8,128)(2,1)} %param.13) | copy-start | bytes 98308
  2.0 13.7 %copy-start = (f32[1,2048]{1,0:T(1,128)S(1)}, f32[1,2048]{1,0:T(1,128)}, u32[]{:S(2)}) copy-start(f32[1,2048]{1,0:T(1,128)} %param.14) | copy-start | bytes 24580
  2.0 13.7 %copy-start.1 = (f32[1,128,4]{1,2,0:T(4,128)S(1)}, f32[1,128,4]{1,2,0:T(4,128)}, u32[]{:S(2)}) copy-start(f32[1,128,4]{1,2,0:T(4,128)} %param.20) | copy-start | bytes 6148
  2.0 13.7 %copy-start.3 = (f32[1,64]{1,0:T(1,128)S(1)}, f32[1,64]{1,0:T(1,128)}, u32[]{:S(2)}) copy-start(f32[1,64]{1,0:T(1,128)} %param.21) | copy-start | bytes 772
  43.0 5.3 %collective-permute-start = (bf16[128,256]{0,1:T(8,128)(2,1)S(1)}, bf16[128,256]{0,1:T(8,128)(2,1)S(1)}, u32[]{:S(2)}, u32[]{:S(2)}) collective-permute-start(bf16[128,256]{0,1:T(8,128)(2,1)S(1)} %get-tuple-element.651), channel_id=1, source_target_pairs={{0,8},{8,16},{16,24},{1,9},{9,17},{17,25},{2,10},{10,18},{18,26},{... | collective-permute-start | bytes 196616 | tf_op jit(solution)/shard_map/while/body/eval_jaxpr/ppermute | solution.py:21
  75.1 6.2 %collective-permute-start = (bf16[128,256]{0,1:T(8,128)(2,1)S(1)}, bf16[128,256]{0,1:T(8,128)(2,1)S(1)}, u32[]{:S(2)}, u32[]{:S(2)}) collective-permute-start(bf16[128,256]{0,1:T(8,128)(2,1)S(1)} %get-tuple-element.651), channel_id=1, source_target_pairs={{0,8},{8,16},{16,24},{1,9},{9,17},{17,25},{2,10},{10,18},{18,26},{... | collective-permute-start | bytes 196616 | tf_op jit(solution)/shard_map/while/body/eval_jaxpr/ppermute | solution.py:21
  108.4 6.2 %collective-permute-start = (bf16[128,256]{0,1:T(8,128)(2,1)S(1)}, bf16[128,256]{0,1:T(8,128)(2,1)S(1)}, u32[]{:S(2)}, u32[]{:S(2)}) collective-permute-start(bf16[128,256]{0,1:T(8,128)(2,1)S(1)} %get-tuple-element.651), channel_id=1, source_target_pairs={{0,8},{8,16},{16,24},{1,9},{9,17},{17,25},{2,10},{10,18},{18,26},{... | collective-permute-start | bytes 196616 | tf_op jit(solution)/shard_map/while/body/eval_jaxpr/ppermute | solution.py:21
  141.6 7.0 %collective-permute-start = (bf16[128,256]{0,1:T(8,128)(2,1)S(1)}, bf16[128,256]{0,1:T(8,128)(2,1)S(1)}, u32[]{:S(2)}, u32[]{:S(2)}) collective-permute-start(bf16[128,256]{0,1:T(8,128)(2,1)S(1)} %get-tuple-element.651), channel_id=1, source_target_pairs={{0,8},{8,16},{16,24},{1,9},{9,17},{17,25},{2,10},{10,18},{18,26},{... | collective-permute-start | bytes 196616 | tf_op jit(solution)/shard_map/while/body/eval_jaxpr/ppermute | solution.py:21
  175.7 7.1 %collective-permute-start = (bf16[128,256]{0,1:T(8,128)(2,1)S(1)}, bf16[128,256]{0,1:T(8,128)(2,1)S(1)}, u32[]{:S(2)}, u32[]{:S(2)}) collective-permute-start(bf16[128,256]{0,1:T(8,128)(2,1)S(1)} %get-tuple-element.651), channel_id=1, source_target_pairs={{0,8},{8,16},{16,24},{1,9},{9,17},{17,25},{2,10},{10,18},{18,26},{... | collective-permute-start | bytes 196616 | tf_op jit(solution)/shard_map/while/body/eval_jaxpr/ppermute | solution.py:21
